TPU v7x, 32 devices: a whole 2x2x4 slice. The times are simulated.
32 devices in a mesh: sp: 8 (over z, x), tp: 4 (over y, core).
Axes of the slice: x: 2, y: 2, z: 4, core: 2. Of those that a mesh axis runs over, the one named last changes fastest.
Arguments:
- result_cotangent_values: bfloat16 [1024, 2048], P('sp'), may hold values from -6 to 6
- specialist_entry_vectors: bfloat16 [1024, 2048], P('sp'), may hold values from -6 to 6
- chosen_specialists: int32 [1024, 2], P('sp'), may hold values from 0 to 3, all different within a row; in each aligned block of 128 rows (0 to 127, 128 to 255, ...) at most 128 rows name the same one
- specialist_mixing_shares: float32 [1024, 2], P('sp'), may hold values from 0.1 to 0.9
- specialist_switch_maps: bfloat16 [8, 2048, 1792], P('sp', None, 'tp'), may hold values from -0.125 to 0.125
- specialist_widen_maps: bfloat16 [8, 2048, 1792], P('sp', None, 'tp'), may hold values from -0.125 to 0.125
- specialist_shrink_maps: bfloat16 [8, 1792, 2048], P('sp', 'tp'), may hold values from -0.09375 to 0.09375
- memory_readout_map: bfloat16 [2048, 2048], P('sp', 'tp'), may hold values from -0.125 to 0.125
- memory_source_vectors: bfloat16 [1024, 2048], P('sp', 'tp'), may hold values from -6 to 6
- memory_hidden_values: bfloat16 [1024, 2048], P('sp', 'tp'), may hold values from -6 to 6
- feature_fading_speed: float32 [2048], P('tp'), may hold values from 1.6276042e-05 to 0.009
- extra_log_fading: float32 [1024], P('sp'), may hold values from -2.8 to 0
- memory_switch_tiles: bfloat16 [8, 256, 256], P('tp'), may hold values from -0.375 to 0.375
- entry_switch_tiles: bfloat16 [8, 256, 256], P('tp'), may hold values from -0.375 to 0.375
Outputs:
- gate_proj_grad: bfloat16 [8, 2048, 1792], P('sp', None, 'tp')
- up_proj_grad: bfloat16 [8, 2048, 1792], P('sp', None, 'tp')
- down_proj_grad: bfloat16 [8, 1792, 2048], P('sp', 'tp')
- out_proj_grad: float32 [2048, 2048], P('sp', 'tp')
- lru_input_grad: float32 [1024, 2048], P('sp', 'tp')
Inputs may be any that keep to these rules, and one draw needn't show every extreme that they name: `chosen_specialists`: each token names two different experts; among the 128 tokens of one device no expert is named more than 128 times, a bound that some block reaches on some device.
All inputs are finite; a program needn't handle non-finite values.
Results may differ from a plain program's by a relative error of at most 0.009.
Values may be sent and summed in bfloat16 or wider, within the bound.
A program may use at most 128 MiB of HBM per device.

v0:
```python
import jax
import jax.numpy as jnp
from jax import lax
from jax.sharding import PartitionSpec as P

SLICES = 2


def prefix(part, axis, combine, identity):
    count = lax.axis_size(axis)
    place = lax.axis_index(axis)
    ahead = count - 1 - place
    gathered = jax.tree.map(lambda a: lax.all_gather(a, axis), part)
    state = jax.tree.map(lambda a, e: jnp.zeros_like(a) + jnp.asarray(e, a.dtype), part, identity)

    def one(turn, state):
        source = count - 1 - turn
        return combine(
            state, jax.tree.map(lambda a: lax.dynamic_index_in_dim(a, source, 0, False), gathered)
        )

    return lax.fori_loop(0, ahead, one, state)


def silu_slope(value):
    sig_value = jax.nn.sigmoid(value)
    return sig_value * (1.0 + value * (1.0 - sig_value))


def compose(upper_map, lower_map):
    return (lower_map[0] * upper_map[0], lower_map[1] + lower_map[0] * upper_map[1])


def chain_join(higher_map, lower_map):
    return (lower_map[0] * higher_map[0], lower_map[1] + lower_map[0] * higher_map[1])


def expert_backward(inputs, grads_in, gate_weight, up_weight, down_weight):
    gate_value = jnp.dot(inputs, gate_weight, preferred_element_type=jnp.float32)
    up_value = jnp.dot(inputs, up_weight, preferred_element_type=jnp.float32)
    active = jax.nn.silu(gate_value)
    hidden = (active * up_value).astype(jnp.bfloat16)
    down_grad = jnp.einsum(
        "rf,rd->fd", hidden, grads_in, preferred_element_type=jnp.float32
    ).astype(jnp.bfloat16)
    hidden_grad = jnp.einsum("rd,fd->rf", grads_in, down_weight, preferred_element_type=jnp.float32)
    gate_grad = (hidden_grad * up_value * silu_slope(gate_value)).astype(jnp.bfloat16)
    up_grad = (hidden_grad * active).astype(jnp.bfloat16)
    gate_weight_grad = jnp.einsum(
        "rd,rf->df", inputs, gate_grad, preferred_element_type=jnp.float32
    ).astype(jnp.bfloat16)
    up_weight_grad = jnp.einsum(
        "rd,rf->df", inputs, up_grad, preferred_element_type=jnp.float32
    ).astype(jnp.bfloat16)
    token_part = jnp.einsum("rf,df->rd", gate_grad, gate_weight, preferred_element_type=jnp.float32)
    token_part = token_part + jnp.einsum(
        "rf,df->rd", up_grad, up_weight, preferred_element_type=jnp.float32
    )
    return (gate_weight_grad, up_weight_grad, down_grad, token_part)


def collect(returned, targets, route_count):
    gathered = jnp.take(returned, targets[0], axis=0).astype(jnp.float32)
    for target in targets[1:]:
        gathered = gathered + jnp.take(returned, target, axis=0).astype(jnp.float32)
    return gathered.reshape(-1, route_count, gathered.shape[-1]).sum(axis=1)


def fill_slots(values, targets, slot_rows):
    buffer = jnp.zeros((slot_rows, values.shape[1]), jnp.bfloat16)
    for target in targets:
        buffer = buffer.at[target].set(values)
    return buffer


def local(
    result_cotangent_values,
    specialist_entry_vectors,
    chosen_specialists,
    specialist_mixing_shares,
    specialist_switch_maps,
    specialist_widen_maps,
    specialist_shrink_maps,
    memory_readout_map,
    memory_source_vectors,
    memory_hidden_values,
    feature_fading_speed,
    extra_log_fading,
    memory_switch_tiles,
    entry_switch_tiles,
):
    tok_rows, feature_count = result_cotangent_values.shape
    route_count = chosen_specialists.shape[1]
    sp_count = lax.axis_size("sp")
    expert_count = sp_count // SLICES
    capacity = min(tok_rows, 4 * tok_rows // expert_count)
    slot_rows = sp_count * capacity
    flat_expert = chosen_specialists.reshape(-1)
    onehot = (flat_expert[:, None] == jnp.arange(expert_count, dtype=jnp.int32)[None, :]).astype(
        jnp.int32
    )
    slot_rank = jnp.sum((jnp.cumsum(onehot, axis=0) - 1) * onehot, axis=1)
    scaled = (
        (
            specialist_mixing_shares[:, :, None]
            * result_cotangent_values[:, None, :].astype(jnp.float32)
        )
        .astype(jnp.bfloat16)
        .reshape(-1, feature_count)
    )
    copies = jnp.broadcast_to(
        specialist_entry_vectors[:, None, :], (tok_rows, route_count, feature_count)
    ).reshape(-1, feature_count)
    targets = [
        (flat_expert * SLICES + slice_index) * capacity + slot_rank for slice_index in range(SLICES)
    ]
    share = feature_count // lax.axis_size("tp")
    first_col = lax.axis_index("tp") * share
    part_grad = lax.dynamic_slice_in_dim(scaled, first_col, share, 1)
    part_rows = lax.dynamic_slice_in_dim(copies, first_col, share, 1)
    send_grad = fill_slots(part_grad, targets, slot_rows)
    send_rows = fill_slots(part_rows, targets, slot_rows)
    got_grad, got_rows = (
        lax.all_to_all(
            send_grad.reshape(sp_count, capacity, share),
            "sp",
            split_axis=0,
            concat_axis=0,
            tiled=True,
        ),
        lax.all_to_all(
            send_rows.reshape(sp_count, capacity, share),
            "sp",
            split_axis=0,
            concat_axis=0,
            tiled=True,
        ),
    )
    recv_grad, recv_rows = (
        lax.all_gather(got_grad, "tp", axis=2, tiled=True),
        lax.all_gather(got_rows, "tp", axis=2, tiled=True),
    )
    inputs = recv_rows.reshape(slot_rows, feature_count)
    grads_in = recv_grad.reshape(slot_rows, feature_count)
    gate_weight_grad, up_weight_grad, down_grad, token_part = expert_backward(
        inputs,
        grads_in,
        specialist_switch_maps[0],
        specialist_widen_maps[0],
        specialist_shrink_maps[0],
    )
    returned = lax.all_to_all(
        token_part.astype(jnp.bfloat16).reshape(sp_count, capacity, feature_count),
        "sp",
        split_axis=0,
        concat_axis=0,
        tiled=True,
    )
    own_sum = collect(returned.reshape(slot_rows, feature_count), targets, route_count)
    moe_grad = lax.psum(own_sum.astype(jnp.bfloat16), "tp").astype(jnp.float32)
    mixed_grad = (result_cotangent_values.astype(jnp.float32) + moe_grad).astype(jnp.bfloat16)
    col_count = memory_readout_map.shape[1]
    columns = mixed_grad
    upstream = jnp.dot(
        columns,
        lax.all_gather(memory_readout_map, "sp", axis=0, tiled=True),
        preferred_element_type=jnp.float32,
    )
    blocks_here = memory_switch_tiles.shape[0]
    block_width = memory_switch_tiles.shape[1]
    blocks_in = memory_source_vectors.reshape(tok_rows, blocks_here, block_width)
    memory_switch_fraction = jax.nn.sigmoid(
        jnp.einsum(
            "tnc,ncd->tnd", blocks_in, memory_switch_tiles, preferred_element_type=jnp.float32
        ).reshape(tok_rows, col_count)
    )
    inp_open = jax.nn.sigmoid(
        jnp.einsum(
            "tnc,ncd->tnd", blocks_in, entry_switch_tiles, preferred_element_type=jnp.float32
        ).reshape(tok_rows, col_count)
    )
    xin = memory_source_vectors.astype(jnp.float32)
    log_fading_factor = (
        -8.0 * memory_switch_fraction * feature_fading_speed[None, :] + extra_log_fading[:, None]
    )
    decay_mult = jnp.exp(log_fading_factor)
    spare_room = -jnp.expm1(2.0 * log_fading_factor)
    in_scale = jnp.sqrt(jnp.maximum(spare_room, 0.01))
    drive = in_scale * inp_open * xin
    coeff = jnp.concatenate([decay_mult[1:], jnp.ones((1, col_count), jnp.float32)], axis=0)
    prod_after, local_part = lax.associative_scan(compose, (coeff, upstream), reverse=True, axis=0)
    alpha_part = decay_mult[0] * local_part[0]
    beta_part = decay_mult[0] * prod_after[0]
    carried = prefix(
        (beta_part, alpha_part),
        "sp",
        chain_join,
        (jnp.ones_like(beta_part), jnp.zeros_like(alpha_part)),
    )
    incoming = carried[1]
    dstate = local_part + prod_after * incoming[None, :]
    scale_slope = jnp.where(spare_room > 0.01, -decay_mult * decay_mult / in_scale, 0.0)
    log_grad = dstate * (
        memory_hidden_values.astype(jnp.float32) - drive + scale_slope * inp_open * xin
    )
    grad_rec = (
        log_grad
        * (-8.0 * feature_fading_speed[None, :])
        * memory_switch_fraction
        * (1.0 - memory_switch_fraction)
    ).astype(jnp.bfloat16)
    grad_in = (dstate * in_scale * xin * inp_open * (1.0 - inp_open)).astype(jnp.bfloat16)
    back_rec = jnp.einsum(
        "tnd,ncd->tnc",
        grad_rec.reshape(tok_rows, blocks_here, block_width),
        memory_switch_tiles,
        preferred_element_type=jnp.float32,
    )
    back_in = jnp.einsum(
        "tnd,ncd->tnc",
        grad_in.reshape(tok_rows, blocks_here, block_width),
        entry_switch_tiles,
        preferred_element_type=jnp.float32,
    )
    lru_input_grad = (
        dstate * in_scale * inp_open
        + back_rec.reshape(tok_rows, col_count)
        + back_in.reshape(tok_rows, col_count)
    )
    columns = mixed_grad
    out_proj_grad = lax.psum_scatter(
        jnp.einsum("tr,tc->rc", columns, memory_hidden_values, preferred_element_type=jnp.float32),
        "sp",
        scatter_dimension=0,
        tiled=True,
    )
    return (
        gate_weight_grad[None],
        up_weight_grad[None],
        down_grad[None],
        out_proj_grad,
        lru_input_grad,
    )


def solution(mesh):
    return jax.shard_map(
        local,
        mesh=mesh,
        in_specs=(
            P("sp", None),
            P("sp", None),
            P("sp", None),
            P("sp", None),
            P("sp", None, "tp"),
            P("sp", None, "tp"),
            P("sp", "tp", None),
            P("sp", "tp"),
            P("sp", "tp"),
            P("sp", "tp"),
            P("tp"),
            P("sp"),
            P("tp", None, None),
            P("tp", None, None),
        ),
        out_specs=(
            P("sp", None, "tp"),
            P("sp", None, "tp"),
            P("sp", "tp", None),
            P("sp", "tp"),
            P("sp", "tp"),
        ),
        check_vma=False,
    )
```

profile of v0, /device:TPU:0, one launch (start us, length us, event | category | flops | bytes accessed | tf_op | source)
XLA Modules:
  0.0 415.6 jit_solution(13920813753677419819)
XLA Ops:
  12.1 1.7 broadcast_in_dim.22
  15.0 3.0 scatter_custom_fusion
  18.0 4.2 %scatter_custom_fusion.1 = bf16[1024,512]{1,0:T(8,128)(2,1)} fusion(bf16[1024,512]{1,0:T(8,128)(2,1)} %scatter_custom_fusion, s32[256]{0:T(256)S(1)} %bitcast.121, bf16[256,2048]{1,0:T(8,128)(2,1)} %reshape.168, s32[]{:T(128)} %constant.77.clone.1, s32[]{:T(128)S(6)} %select_n.47), kind=kCustom, calls=%fused_computation.72 | custom fusion | bytes 1311236 | tf_op jit(solution)/shard_map/scatter | solution.py:72
  22.3 33.3 %all_to_all.15 = bf16[8,128,512]{2,1,0:T(8,128)(2,1)} all-to-all(bf16[8,128,512]{2,1,0:T(8,128)(2,1)} %bitcast.7), channel_id=1, replica_groups=mesh['sp'=8,'tp'=4] {'sp'}, dimensions={0} | all-to-all | bytes 2097152 | tf_op jit(solution)/shard_map/all_to_all | solution.py:131
  55.6 2.4 mul.275
  58.1 3.8 mul.276
  62.1 3.3 scatter_custom_fusion.2
  65.4 4.4 %scatter_custom_fusion.3 = bf16[1024,512]{1,0:T(8,128)(2,1)} fusion(bf16[1024,512]{1,0:T(8,128)(2,1)} %scatter_custom_fusion.2, s32[256]{0:T(256)S(1)} %bitcast.122, f32[256,2048]{1,0:T(8,128)} %mul.276, s32[]{:T(128)S(6)} %select_n.47, f32[256]{0:T(256)S(1)} %mul.273), kind=kCustom, calls=%fused_computation.154 | custom fusion | flops 262144 | bytes 1573892 | tf_op jit(solution)/shard_map/scatter | solution.py:72
  69.8 29.7 %all_to_all.16 = bf16[8,128,512]{2,1,0:T(8,128)(2,1)} all-to-all(bf16[8,128,512]{2,1,0:T(8,128)(2,1)} %bitcast.106), channel_id=1, replica_groups=mesh['sp'=8,'tp'=4] {'sp'}, dimensions={0} | all-to-all | bytes 2097152 | tf_op jit(solution)/shard_map/all_to_all | solution.py:124
  99.5 5.7 %fusion.5 = f32[1024,448]{0,1:T(8,128)} fusion(bf16[1024,2048]{1,0:T(8,128)(2,1)} %bitcast.125, bf16[1,2048,448]{1,2,0:T(8,128)(2,1)S(1)} %copy-done), kind=kOutput, calls=%fused_computation.19 | convolution fusion | flops 1879048192 | bytes 7864320 | tf_op jit(solution)/shard_map/dot_general | solution.py:39
  105.2 3.4 fusion.8
  108.5 24.5 %all-gather.8.cloned.1.call-done = bf16[8,128,2048]{2,1,0:T(8,128)(2,1)} async-done(((bf16[8,128,512]{2,1,0:T(8,128)(2,1)}), bf16[8,128,2048]{2,1,0:T(8,128)(2,1)}) %all-gather.8.cloned.1.call-update) | async-done | bytes 4194320 | tf_op jit(solution)/shard_map/all_gather | solution.py:140
  133.1 6.4 %multiply_convert_fusion.1 = (bf16[1024,448]{0,1:T(8,128)(2,1)S(1)}, bf16[1024,448]{0,1:T(8,128)(2,1)S(1)}) fusion(f32[1024,448]{0,1:T(8,128)} %fusion.5, f32[1024,448]{0,1:T(8,128)} %fusion.8, bf16[1024,2048]{1,0:T(8,128)(2,1)} %bitcast.129, bf16[1,448,2048]{2,1,0:T(8,128)(2,1)} %param.24), kind=kOutput, calls=%fused_computation.27 | convolution fusion | flops 1885011968 | bytes 11534336 | tf_op jit(solution)/shard_map/rd,fd->rf/dot_general | solution.py:46
  139.5 2.4 fusion.3
  142.0 4.5 %add_convert_fusion = bf16[1024,2048]{1,0:T(8,128)(2,1)} fusion(f32[1024,2048]{1,0:T(8,128)S(1)} %fusion.3, bf16[1024,448]{0,1:T(8,128)(2,1)S(1)} %get-tuple-element.109, bf16[1,2048,448]{1,2,0:T(8,128)(2,1)S(1)} %copy-done.15), kind=kOutput, calls=%fused_computation.9 | convolution fusion | flops 1883242496 | bytes 15335424 | tf_op jit(solution)/shard_map/rf,df->rd/dot_general | solution.py:56
  146.5 5.5 %all-to-all-start.2 = ((bf16[8,128,2048]{2,1,0:T(8,128)(2,1)}), bf16[8,128,2048]{2,1,0:T(8,128)(2,1)}, u32[]{:S(2)}, u32[]{:S(2)}) async-start(bf16[8,128,2048]{2,1,0:T(8,128)(2,1)} %bitcast.105), calls=%async_computation.2 | async-start | bytes 8388608 | tf_op jit(solution)/shard_map/all_to_all | solution.py:152
  152.2 93.4 %all-to-all-done.2 = bf16[8,128,2048]{2,1,0:T(8,128)(2,1)} async-done(((bf16[8,128,2048]{2,1,0:T(8,128)(2,1)}), bf16[8,128,2048]{2,1,0:T(8,128)(2,1)}, u32[]{:S(2)}, u32[]{:S(2)}) %all-to-all-start.2) | async-done | bytes 4194336 | tf_op jit(solution)/shard_map/all_to_all | solution.py:152
  245.7 6.1 %gather_fusion.1 = bf16[256,2048]{1,0:T(8,128)(2,1)} fusion(bf16[1024,2048]{1,0:T(8,128)(2,1)} %bitcast.18, s32[1024]{0:T(1024)S(1)} %get-tuple-element.150), kind=kCustom, calls=%fused_computation.1.clone | custom fusion | bytes 2098176 | tf_op jit(solution)/shard_map/jit(_take)/gather | solution.py:65
  251.7 6.1 %gather_fusion = bf16[256,2048]{1,0:T(8,128)(2,1)} fusion(bf16[1024,2048]{1,0:T(8,128)(2,1)} %bitcast.18, s32[1024]{0:T(1024)S(1)} %get-tuple-element.151), kind=kCustom, calls=%fused_computation.clone | custom fusion | bytes 2098176 | tf_op jit(solution)/shard_map/jit(_take)/gather | solution.py:63
  257.8 1.9 convert_add_fusion
  259.7 2.3 reshape.175
  262.0 5.0 %reduce_sum.22 = bf16[128,2048]{1,0:T(8,128)(2,1)} reduce(f32[128,2,2048]{2,1,0:T(2,128)} %reshape.175, f32[]{:T(128)} %constant.87.clone.1), dimensions={1}, to_apply=%region_7.9 | reduce | flops 262144 | bytes 2621444 | tf_op jit(solution)/shard_map/reduce_sum | solution.py:66
  269.8 5.9 %fusion.1 = bf16[1,2048,448]{1,2,0:T(8,128)(2,1)} fusion(bf16[1024,448]{0,1:T(8,128)(2,1)} %copy-done.16, bf16[1024,2048]{1,0:T(8,128)(2,1)} %bitcast.126), kind=kOutput, calls=%fused_computation.14 | convolution fusion | flops 1879965696 | bytes 6946816 | tf_op jit(solution)/shard_map/rd,rf->df/dot_general | solution.py:49
  275.7 23.1 %all-reduce.32.cloned.1.call-done = bf16[128,2048]{1,0:T(8,128)(2,1)} async-done(((bf16[128,2048]{1,0:T(8,128)(2,1)}), bf16[128,2048]{1,0:T(8,128)(2,1)}) %all-reduce.32.cloned.1.call-update) | async-done | bytes 524304 | tf_op jit(solution)/shard_map/psum | solution.py:160
  298.8 3.8 fusion.44
  303.8 5.6 %fusion.2 = bf16[1,2048,448]{1,2,0:T(8,128)(2,1)} fusion(bf16[1024,448]{0,1:T(8,128)(2,1)S(1)} %copy-done.18, bf16[1024,2048]{1,0:T(8,128)(2,1)} %bitcast.127), kind=kOutput, calls=%fused_computation.15 | convolution fusion | flops 1879965696 | bytes 6946816 | tf_op jit(solution)/shard_map/rd,rf->df/dot_general | solution.py:52
  309.4 3.4 fusion
  312.8 4.0 all-gather.10.cloned.1.call-done
  316.8 2.0 fusion.43
  322.1 27.2 %all-gather = f32[8,1,512]{2,1,0:T(1,128)S(1)} all-gather(f32[1,1,512]{2,1,0:T(1,128)S(1)} %get-tuple-element.113), channel_id=1, replica_groups=mesh['sp'=8,'tp'=4] {'sp'}, dimensions={0}, use_global_device_ids=true | all-gather | bytes 18432 | tf_op jit(solution)/shard_map/all_gather | solution.py:13
  349.3 26.6 %all-gather.1 = f32[8,1,512]{2,1,0:T(1,128)S(1)} all-gather(f32[1,1,512]{2,1,0:T(1,128)S(1)} %get-tuple-element.112), channel_id=1, replica_groups=mesh['sp'=8,'tp'=4] {'sp'}, dimensions={0}, use_global_device_ids=true | all-gather | bytes 18432 | tf_op jit(solution)/shard_map/all_gather | solution.py:13
  378.1 30.1 %reduce-scatter.2.cloned.1.call-done = f32[256,512]{1,0:T(8,128)} async-done(((f32[2048,512]{1,0:T(8,128)}), f32[256,512]{1,0:T(8,128)}) %reduce-scatter.2.cloned.1.call-update) | async-done | bytes 524304 | tf_op jit(solution)/shard_map/reduce_scatter | solution.py:231
  (223 shorter events, 14.6 us)
Async XLA Ops:
  8.0 91.5 %copy-start = (bf16[1,2048,448]{1,2,0:T(8,128)(2,1)S(1)}, bf16[1,2048,448]{1,2,0:T(8,128)(2,1)}, u32[]{:S(2)}) copy-start(bf16[1,2048,448]{1,2,0:T(8,128)(2,1)} %param.22) | copy-start | bytes 5505028
  8.0 91.5 %all-gather.6.cloned.1.call-start = ((), (), s32[]{:S(2)}) async-start(), calls=%async_computation.4 | async-start | bytes 5242880 | tf_op jit(solution)/shard_map/all_gather | solution.py:141
  22.3 33.4 %copy-start.2 = (bf16[128,2048]{1,0:T(8,128)(2,1)S(1)}, bf16[128,2048]{1,0:T(8,128)(2,1)}, u32[]{:S(2)}) copy-start(bf16[128,2048]{1,0:T(8,128)(2,1)} %param.18) | copy-start | bytes 1572868
  55.6 77.5 %all-gather.8.cloned.1.call-start = ((), (), s32[]{:S(2)}) async-start(), calls=%async_computation.5 | async-start | bytes 5242880 | tf_op jit(solution)/shard_map/all_gather | solution.py:140
  58.1 3.8 copy-start.11
  99.5 5.7 %copy-start.12 = (bf16[8,128,2048]{2,1,0:T(8,128)(2,1)S(1)}, bf16[8,128,2048]{2,1,0:T(8,128)(2,1)}, u32[]{:S(2)}) copy-start(bf16[8,128,2048]{2,1,0:T(8,128)(2,1)} %all-gather.6.cloned.1.call-done) | copy-start | bytes 12582916
  99.5 5.7 %copy-start.14 = (bf16[1,2048,448]{1,2,0:T(8,128)(2,1)S(1)}, bf16[1,2048,448]{1,2,0:T(8,128)(2,1)}, u32[]{:S(2)}) copy-start(bf16[1,2048,448]{1,2,0:T(8,128)(2,1)} %param.23) | copy-start | bytes 5505028
  139.5 2.5 copy-start.16
  139.5 2.5 copy-start.17
  139.5 2.5 copy-start.15
  146.5 99.2 %all-to-all-start.2 = ((bf16[8,128,2048]{2,1,0:T(8,128)(2,1)}), bf16[8,128,2048]{2,1,0:T(8,128)(2,1)}, u32[]{:S(2)}, u32[]{:S(2)}) async-start(bf16[8,128,2048]{2,1,0:T(8,128)(2,1)} %bitcast.105), calls=%async_computation.2 | async-start | bytes 8388608 | tf_op jit(solution)/shard_map/all_to_all | solution.py:152
  152.0 146.8 %all-reduce.32.cloned.1.call-start = ((), (), s32[]{:S(2)}) async-start(), calls=%async_computation.6 | async-start | bytes 1048576 | tf_op jit(solution)/shard_map/psum | solution.py:160
  262.0 5.9 %copy-start.6 = (bf16[2,256,256]{2,1,0:T(8,128)(2,1)S(1)}, bf16[2,256,256]{2,1,0:T(8,128)(2,1)}, u32[]{:S(2)}) copy-start(bf16[2,256,256]{2,1,0:T(8,128)(2,1)} %param.30) | copy-start | bytes 786436
  262.0 5.9 %copy-start.7 = (bf16[128,512]{1,0:T(8,128)(2,1)S(1)}, bf16[128,512]{1,0:T(8,128)(2,1)}, u32[]{:S(2)}) copy-start(bf16[128,512]{1,0:T(8,128)(2,1)} %param.26) | copy-start | bytes 393220
  267.1 1.3 copy-start.9
  267.1 1.4 copy-start.10
  267.1 49.7 %all-gather.10.cloned.1.call-start = ((), (), s32[]{:S(2)}) async-start(), calls=%async_computation.8 | async-start | bytes 2359296 | tf_op jit(solution)/shard_map/all_gather | solution.py:166
  267.7 140.6 %reduce-scatter.2.cloned.1.call-start = ((), (), s32[]{:S(2)}) async-start(), calls=%async_computation.7 | async-start | bytes 4718592 | tf_op jit(solution)/shard_map/reduce_scatter | solution.py:231
  267.9 1.0 copy-start.5
  269.8 29.0 %copy-start.4 = (bf16[128,512]{1,0:T(8,128)(2,1)S(1)}, bf16[128,512]{1,0:T(8,128)(2,1)}, u32[]{:S(2)}) copy-start(bf16[128,512]{1,0:T(8,128)(2,1)} %param.27) | copy-start | bytes 393220
  302.6 1.2 copy-start.18
  303.7 5.6 %copy-start.13 = (bf16[8,128,2048]{2,1,0:T(8,128)(2,1)S(1)}, bf16[8,128,2048]{2,1,0:T(8,128)(2,1)}, u32[]{:S(2)}) copy-start(bf16[8,128,2048]{2,1,0:T(8,128)(2,1)} %all-gather.8.cloned.1.call-done) | copy-start | bytes 12582916
  303.7 5.6 %copy-start.19 = (f32[1024,448]{0,1:T(8,128)S(1)}, f32[1024,448]{0,1:T(8,128)}, u32[]{:S(2)}) copy-start(f32[1024,448]{0,1:T(8,128)} %fusion.5) | copy-start | bytes 5505028
  303.8 5.6 %copy-start.20 = (f32[1024,448]{0,1:T(8,128)S(1)}, f32[1024,448]{0,1:T(8,128)}, u32[]{:S(2)}) copy-start(f32[1024,448]{0,1:T(8,128)} %fusion.8) | copy-start | bytes 5505028
  309.4 7.4 %copy-start.3 = (bf16[128,2048]{1,0:T(8,128)(2,1)S(1)}, bf16[128,2048]{1,0:T(8,128)(2,1)}, u32[]{:S(2)}) copy-start(bf16[128,2048]{1,0:T(8,128)(2,1)} %all-reduce.32.cloned.1.call-done) | copy-start | bytes 1572868
  321.6 54.7 %copy-start.8 = (bf16[128,512]{1,0:T(8,128)(2,1)S(1)}, bf16[128,512]{1,0:T(8,128)(2,1)}, u32[]{:S(2)}) copy-start(bf16[128,512]{1,0:T(8,128)(2,1)} %param.26) | copy-start | bytes 393220
  376.8 31.4 %copy-start.1 = (bf16[1,2048,448]{1,2,0:T(8,128)(2,1)S(1)}, bf16[1,2048,448]{1,2,0:T(8,128)(2,1)}, u32[]{:S(2)}) copy-start(bf16[1,2048,448]{1,2,0:T(8,128)(2,1)} %param.22) | copy-start | bytes 5505028
Sparse Core Ops, SparseCore 0:
  55.7 33.4 all-gather.5
  99.6 33.4 all-gather.7
  267.2 31.5 all-reduce.31
Sparse Core Ops, SparseCore 1:
  269.7 47.0 all-gather.9
  320.8 87.3 reduce-scatter.1
where the time goes:
time: 423 us; the launch traced here: 416 us
  waiting for transfers between devices  176 us (42%)
  blocking collectives  117 us (28%)
  matrix products  44.1 us (10%)
  local copies, waits for them, and re-layouts  37.3 us (9%)
  other arithmetic  18.9 us (4%)
  between operations  16.5 us (4%)
  starting transfers between devices  6.08 us (1%)
    all_to_all x1, waiting for transfers between devices, local(): lax.all_to_all(token_part.astype(jnp.bfloat16).reshape(sp_count, capacity...  93.4 us
    all_gather x2, blocking collectives, prefix(): gathered = jax.tree.map(lambda a: lax.all_gather(a, axis), part)  53.8 us
    all_to_all x1, blocking collectives, local(): lax.all_to_all(send_rows.reshape(sp_count, capacity, share), 'sp', split_...  33.3 us
    reduce_scatter x1, waiting for transfers between devices, local(): lax.psum_scatter(jnp.einsum('tr,tc->rc', columns, memory_hidden_values, p...  30.1 us
    all_to_all x1, blocking collectives, local(): lax.all_to_all(send_grad.reshape(sp_count, capacity, share), 'sp', split_...  29.7 us
    all_gather x1, waiting for transfers between devices, local(): lax.all_gather(got_grad, 'tp', axis=2, tiled=True)  24.5 us
    psum x1, waiting for transfers between devices, local(): moe_grad = lax.psum(own_sum.astype(jnp.bfloat16), 'tp').astype(jnp.float32)  23.1 us
  transfers between devices with their start and end apart: 6, of which 5 were waited for; matrix products, arithmetic and copies ran while one was open for 12% of the time, Pallas kernels for 0%

commit v1 on v0

--- a/solution.py
+++ b/solution.py
@@ -4,6 +4,12 @@
 from jax.sharding import PartitionSpec as P
 
 SLICES = 2
+
+
+def add_all(x, axis):
+    parts = lax.all_gather(x, axis, axis=0, tiled=False)
+    total = parts.sum(axis=0)
+    return total
 
 
 def prefix(part, axis, combine, identity):
@@ -157,7 +163,7 @@
         tiled=True,
     )
     own_sum = collect(returned.reshape(slot_rows, feature_count), targets, route_count)
-    moe_grad = lax.psum(own_sum.astype(jnp.bfloat16), "tp").astype(jnp.float32)
+    moe_grad = add_all(own_sum.astype(jnp.bfloat16), "tp").astype(jnp.float32)
     mixed_grad = (result_cotangent_values.astype(jnp.float32) + moe_grad).astype(jnp.bfloat16)
     col_count = memory_readout_map.shape[1]
     columns = mixed_grad

time: 423 us -> 444 us (1.050)
  waiting for transfers between devices: 176 us -> 198 us
    all_gather x1, waiting for transfers between devices: 4 us -> 37 us  [local(): lax.all_gather(memory_readout_map, 'sp', axis=0, tiled=True)]
    psum x1 -> x0, waiting for transfers between devices: 23.1 us -> none  [local(): moe_grad = lax.psum(own_sum.astype(jnp.bfloat16), 'tp').astype(jnp.float32)]
    all_gather x0 -> x1, waiting for transfers between devices: none -> 12.1 us  [add_all(): parts = lax.all_gather(x, axis, axis=0, tiled=False)]
where the time goes in v1:
time: 444 us; the launch traced here: 436 us
  waiting for transfers between devices  198 us (45%)
  blocking collectives  117 us (26%)
  matrix products  43.4 us (10%)
  local copies, waits for them, and re-layouts  36.1 us (8%)
  other arithmetic  21 us (5%)
  between operations  15.1 us (3%)
  starting transfers between devices  6.1 us (1%)
    all_to_all x1, waiting for transfers between devices, local(): lax.all_to_all(token_part.astype(jnp.bfloat16).reshape(sp_count, capacity...  93.4 us
    all_gather x2, blocking collectives, prefix(): gathered = jax.tree.map(lambda a: lax.all_gather(a, axis), part)  53.8 us
    all_gather x1, waiting for transfers between devices, local(): lax.all_gather(memory_readout_map, 'sp', axis=0, tiled=True)  37 us
    all_to_all x1, blocking collectives, local(): lax.all_to_all(send_rows.reshape(sp_count, capacity, share), 'sp', split_...  33.3 us
    reduce_scatter x1, waiting for transfers between devices, local(): lax.psum_scatter(jnp.einsum('tr,tc->rc', columns, memory_hidden_values, p...  30.1 us
    all_to_all x1, blocking collectives, local(): lax.all_to_all(send_grad.reshape(sp_count, capacity, share), 'sp', split_...  29.7 us
    all_gather x1, waiting for transfers between devices, local(): lax.all_gather(got_grad, 'tp', axis=2, tiled=True)  24.5 us
    all_gather x1, waiting for transfers between devices, add_all(): parts = lax.all_gather(x, axis, axis=0, tiled=False)  12.1 us
  transfers between devices with their start and end apart: 6, of which 5 were waited for; matrix products, arithmetic and copies ran while one was open for 12% of the time, Pallas kernels for 0%

profile of v1, /device:TPU:0, one launch (start us, length us, event | category | flops | bytes accessed | tf_op | source)
XLA Modules:
  0.0 436.3 jit_solution(13711979868662004435)
XLA Ops:
  14.2 3.0 scatter_custom_fusion
  17.2 4.2 scatter_custom_fusion.1
  21.4 33.3 %all_to_all.15 = bf16[8,128,512]{2,1,0:T(8,128)(2,1)} all-to-all(bf16[8,128,512]{2,1,0:T(8,128)(2,1)} %bitcast.7), channel_id=1, replica_groups=mesh['sp'=8,'tp'=4] {'sp'}, dimensions={0} | all-to-all | bytes 2097152 | tf_op jit(solution)/shard_map/all_to_all | solution.py:137
  54.8 2.4 mul.275
  57.2 3.8 mul.276
  61.3 3.3 scatter_custom_fusion.2
  64.5 4.4 %scatter_custom_fusion.3 = bf16[1024,512]{1,0:T(8,128)(2,1)} fusion(bf16[1024,512]{1,0:T(8,128)(2,1)} %scatter_custom_fusion.2, s32[256]{0:T(256)S(1)} %bitcast.124, f32[256,2048]{1,0:T(8,128)} %mul.276, s32[]{:T(128)S(6)} %select_n.47, f32[256]{0:T(256)S(1)} %mul.273), kind=kCustom, calls=%fused_computation.154 | custom fusion | flops 262144 | bytes 1573892 | tf_op jit(solution)/shard_map/scatter | solution.py:78
  68.9 29.7 %all_to_all.16 = bf16[8,128,512]{2,1,0:T(8,128)(2,1)} all-to-all(bf16[8,128,512]{2,1,0:T(8,128)(2,1)} %bitcast.107), channel_id=1, replica_groups=mesh['sp'=8,'tp'=4] {'sp'}, dimensions={0} | all-to-all | bytes 2097152 | tf_op jit(solution)/shard_map/all_to_all | solution.py:130
  98.7 5.7 %fusion.5 = f32[1024,448]{0,1:T(8,128)} fusion(bf16[1024,2048]{1,0:T(8,128)(2,1)} %bitcast.127, bf16[1,2048,448]{1,2,0:T(8,128)(2,1)S(1)} %copy-done), kind=kOutput, calls=%fused_computation.19 | convolution fusion | flops 1879048192 | bytes 7864320 | tf_op jit(solution)/shard_map/dot_general | solution.py:45
  104.3 3.4 fusion.8
  107.7 24.5 %all-gather.10.cloned.1.call-done = bf16[8,128,2048]{2,1,0:T(8,128)(2,1)} async-done(((bf16[8,128,512]{2,1,0:T(8,128)(2,1)}), bf16[8,128,2048]{2,1,0:T(8,128)(2,1)}) %all-gather.10.cloned.1.call-update) | async-done | bytes 4194320 | tf_op jit(solution)/shard_map/all_gather | solution.py:146
  132.2 6.4 %multiply_convert_fusion.1 = (bf16[1024,448]{0,1:T(8,128)(2,1)S(1)}, bf16[1024,448]{0,1:T(8,128)(2,1)S(1)}) fusion(f32[1024,448]{0,1:T(8,128)} %fusion.5, f32[1024,448]{0,1:T(8,128)} %fusion.8, bf16[1024,2048]{1,0:T(8,128)(2,1)} %bitcast.131, bf16[1,448,2048]{2,1,0:T(8,128)(2,1)} %param.24), kind=kOutput, calls=%fused_computation.27 | convolution fusion | flops 1885011968 | bytes 11534336 | tf_op jit(solution)/shard_map/rd,fd->rf/dot_general | solution.py:52
  138.7 2.4 fusion.3
  141.1 4.5 %add_convert_fusion = bf16[1024,2048]{1,0:T(8,128)(2,1)} fusion(f32[1024,2048]{1,0:T(8,128)S(1)} %fusion.3, bf16[1024,448]{0,1:T(8,128)(2,1)S(1)} %get-tuple-element.109, bf16[1,2048,448]{1,2,0:T(8,128)(2,1)S(1)} %copy-done.13), kind=kOutput, calls=%fused_computation.9 | convolution fusion | flops 1883242496 | bytes 15335424 | tf_op jit(solution)/shard_map/rf,df->rd/dot_general | solution.py:62
  145.6 5.5 %all-to-all-start.2 = ((bf16[8,128,2048]{2,1,0:T(8,128)(2,1)}), bf16[8,128,2048]{2,1,0:T(8,128)(2,1)}, u32[]{:S(2)}, u32[]{:S(2)}) async-start(bf16[8,128,2048]{2,1,0:T(8,128)(2,1)} %bitcast.106), calls=%async_computation.2 | async-start | bytes 8388608 | tf_op jit(solution)/shard_map/all_to_all | solution.py:158
  151.4 93.4 %all-to-all-done.2 = bf16[8,128,2048]{2,1,0:T(8,128)(2,1)} async-done(((bf16[8,128,2048]{2,1,0:T(8,128)(2,1)}), bf16[8,128,2048]{2,1,0:T(8,128)(2,1)}, u32[]{:S(2)}, u32[]{:S(2)}) %all-to-all-start.2) | async-done | bytes 4194336 | tf_op jit(solution)/shard_map/all_to_all | solution.py:158
  244.9 6.1 %gather_fusion.1 = bf16[256,2048]{1,0:T(8,128)(2,1)} fusion(bf16[1024,2048]{1,0:T(8,128)(2,1)} %bitcast.18, s32[1024]{0:T(1024)S(1)} %get-tuple-element.150), kind=kCustom, calls=%fused_computation.1.clone | custom fusion | bytes 2098176 | tf_op jit(solution)/shard_map/jit(_take)/gather | solution.py:71
  250.9 6.1 %gather_fusion = bf16[256,2048]{1,0:T(8,128)(2,1)} fusion(bf16[1024,2048]{1,0:T(8,128)(2,1)} %bitcast.18, s32[1024]{0:T(1024)S(1)} %get-tuple-element.151), kind=kCustom, calls=%fused_computation.clone | custom fusion | bytes 2098176 | tf_op jit(solution)/shard_map/jit(_take)/gather | solution.py:69
  257.0 1.9 convert_add_fusion
  258.9 2.3 reshape.183
  261.2 5.0 %reduce_sum.34 = bf16[128,2048]{1,0:T(8,128)(2,1)} reduce(f32[128,2,2048]{2,1,0:T(2,128)} %reshape.183, f32[]{:T(128)} %constant.88.clone.1), dimensions={1}, to_apply=%region_7.9 | reduce | flops 262144 | bytes 2621444 | tf_op jit(solution)/shard_map/reduce_sum | solution.py:72
  269.0 6.0 %fusion.1 = bf16[1,2048,448]{1,2,0:T(8,128)(2,1)} fusion(bf16[1024,448]{0,1:T(8,128)(2,1)} %copy-done.14, bf16[1024,2048]{1,0:T(8,128)(2,1)} %bitcast.128), kind=kOutput, calls=%fused_computation.14 | convolution fusion | flops 1879965696 | bytes 6946816 | tf_op jit(solution)/shard_map/rd,rf->df/dot_general | solution.py:55
  275.0 12.1 %all-gather.14.cloned.1.call-done = bf16[512,2048]{1,0:T(8,128)(2,1)} async-done(((bf16[128,2048]{1,0:T(8,128)(2,1)}), bf16[512,2048]{1,0:T(8,128)(2,1)}) %all-gather.14.cloned.1.call-update) | async-done | bytes 2097168 | tf_op jit(solution)/shard_map/all_gather | solution.py:10
  287.1 2.0 reduce_sum.35
  289.1 2.7 fusion.44
  291.9 5.9 %fusion.2 = bf16[1,2048,448]{1,2,0:T(8,128)(2,1)} fusion(bf16[1024,448]{0,1:T(8,128)(2,1)} %copy-done.15, bf16[1024,2048]{1,0:T(8,128)(2,1)} %bitcast.129), kind=kOutput, calls=%fused_computation.15 | convolution fusion | flops 1879965696 | bytes 6946816 | tf_op jit(solution)/shard_map/rd,rf->df/dot_general | solution.py:58
  297.9 3.4 fusion
  301.2 37.0 %all-gather.12.cloned.1.call-done = bf16[2048,512]{1,0:T(8,128)(2,1)} async-done(((bf16[256,512]{1,0:T(8,128)(2,1)}), bf16[2048,512]{1,0:T(8,128)(2,1)}) %all-gather.12.cloned.1.call-update) | async-done | bytes 2097168 | tf_op jit(solution)/shard_map/all_gather | solution.py:172
  338.2 2.0 fusion.43
  343.5 27.1 %all-gather.1 = f32[8,1,512]{2,1,0:T(1,128)S(1)} all-gather(f32[1,1,512]{2,1,0:T(1,128)S(1)} %get-tuple-element.113), channel_id=1, replica_groups=mesh['sp'=8,'tp'=4] {'sp'}, dimensions={0}, use_global_device_ids=true | all-gather | bytes 18432 | tf_op jit(solution)/shard_map/all_gather | solution.py:19
  370.7 26.6 %all-gather.2 = f32[8,1,512]{2,1,0:T(1,128)S(1)} all-gather(f32[1,1,512]{2,1,0:T(1,128)S(1)} %get-tuple-element.112), channel_id=1, replica_groups=mesh['sp'=8,'tp'=4] {'sp'}, dimensions={0}, use_global_device_ids=true | all-gather | bytes 18432 | tf_op jit(solution)/shard_map/all_gather | solution.py:19
  399.5 30.1 %reduce-scatter.2.cloned.1.call-done = f32[256,512]{1,0:T(8,128)} async-done(((f32[2048,512]{1,0:T(8,128)}), f32[256,512]{1,0:T(8,128)}) %reduce-scatter.2.cloned.1.call-update) | async-done | bytes 524304 | tf_op jit(solution)/shard_map/reduce_scatter | solution.py:237
  (218 shorter events, 15.1 us)
Async XLA Ops:
  7.2 91.5 %copy-start = (bf16[1,2048,448]{1,2,0:T(8,128)(2,1)S(1)}, bf16[1,2048,448]{1,2,0:T(8,128)(2,1)}, u32[]{:S(2)}) copy-start(bf16[1,2048,448]{1,2,0:T(8,128)(2,1)} %param.22) | copy-start | bytes 5505028
  7.2 91.5 %all-gather.8.cloned.1.call-start = ((), (), s32[]{:S(2)}) async-start(), calls=%async_computation.4 | async-start | bytes 5242880 | tf_op jit(solution)/shard_map/all_gather | solution.py:147
  21.4 33.4 %copy-start.2 = (bf16[128,2048]{1,0:T(8,128)(2,1)S(1)}, bf16[128,2048]{1,0:T(8,128)(2,1)}, u32[]{:S(2)}) copy-start(bf16[128,2048]{1,0:T(8,128)(2,1)} %param.18) | copy-start | bytes 1572868
  54.7 77.5 %all-gather.10.cloned.1.call-start = ((), (), s32[]{:S(2)}) async-start(), calls=%async_computation.5 | async-start | bytes 5242880 | tf_op jit(solution)/shard_map/all_gather | solution.py:146
  57.2 3.8 copy-start.9
  98.7 5.7 %copy-start.10 = (bf16[8,128,2048]{2,1,0:T(8,128)(2,1)S(1)}, bf16[8,128,2048]{2,1,0:T(8,128)(2,1)}, u32[]{:S(2)}) copy-start(bf16[8,128,2048]{2,1,0:T(8,128)(2,1)} %all-gather.8.cloned.1.call-done) | copy-start | bytes 12582916
  98.7 5.7 %copy-start.12 = (bf16[1,2048,448]{1,2,0:T(8,128)(2,1)S(1)}, bf16[1,2048,448]{1,2,0:T(8,128)(2,1)}, u32[]{:S(2)}) copy-start(bf16[1,2048,448]{1,2,0:T(8,128)(2,1)} %param.23) | copy-start | bytes 5505028
  138.6 2.5 copy-start.14
  138.6 2.5 copy-start.15
  138.6 2.5 copy-start.13
  145.6 99.2 %all-to-all-start.2 = ((bf16[8,128,2048]{2,1,0:T(8,128)(2,1)}), bf16[8,128,2048]{2,1,0:T(8,128)(2,1)}, u32[]{:S(2)}, u32[]{:S(2)}) async-start(bf16[8,128,2048]{2,1,0:T(8,128)(2,1)} %bitcast.106), calls=%async_computation.2 | async-start | bytes 8388608 | tf_op jit(solution)/shard_map/all_to_all | solution.py:158
  151.2 135.9 %all-gather.14.cloned.1.call-start = ((), (), s32[]{:S(2)}) async-start(), calls=%async_computation.8 | async-start | bytes 2621440 | tf_op jit(solution)/shard_map/all_gather | solution.py:10
  261.2 5.9 %copy-start.5 = (bf16[2,256,256]{2,1,0:T(8,128)(2,1)S(1)}, bf16[2,256,256]{2,1,0:T(8,128)(2,1)}, u32[]{:S(2)}) copy-start(bf16[2,256,256]{2,1,0:T(8,128)(2,1)} %param.30) | copy-start | bytes 786436
  261.2 5.9 %copy-start.6 = (bf16[128,512]{1,0:T(8,128)(2,1)S(1)}, bf16[128,512]{1,0:T(8,128)(2,1)}, u32[]{:S(2)}) copy-start(bf16[128,512]{1,0:T(8,128)(2,1)} %param.26) | copy-start | bytes 393220
  266.2 1.3 copy-start.7
  266.2 1.4 copy-start.8
  266.3 71.9 %all-gather.12.cloned.1.call-start = ((), (), s32[]{:S(2)}) async-start(), calls=%async_computation.7 | async-start | bytes 2359296 | tf_op jit(solution)/shard_map/all_gather | solution.py:172
  266.8 162.7 %reduce-scatter.2.cloned.1.call-start = ((), (), s32[]{:S(2)}) async-start(), calls=%async_computation.6 | async-start | bytes 4718592 | tf_op jit(solution)/shard_map/reduce_scatter | solution.py:237
  267.1 1.0 copy-start.4
  275.0 14.2 %copy-start.3 = (bf16[128,512]{1,0:T(8,128)(2,1)S(1)}, bf16[128,512]{1,0:T(8,128)(2,1)}, u32[]{:S(2)}) copy-start(bf16[128,512]{1,0:T(8,128)(2,1)} %param.27) | copy-start | bytes 393220
  291.9 5.9 %copy-start.11 = (bf16[8,128,2048]{2,1,0:T(8,128)(2,1)S(1)}, bf16[8,128,2048]{2,1,0:T(8,128)(2,1)}, u32[]{:S(2)}) copy-start(bf16[8,128,2048]{2,1,0:T(8,128)(2,1)} %all-gather.10.cloned.1.call-done) | copy-start | bytes 12582916
  291.9 5.9 %copy-start.16 = (f32[1024,448]{0,1:T(8,128)S(1)}, f32[1024,448]{0,1:T(8,128)}, u32[]{:S(2)}) copy-start(f32[1024,448]{0,1:T(8,128)} %fusion.5) | copy-start | bytes 5505028
  291.9 5.9 %copy-start.17 = (f32[1024,448]{0,1:T(8,128)S(1)}, f32[1024,448]{0,1:T(8,128)}, u32[]{:S(2)}) copy-start(f32[1024,448]{0,1:T(8,128)} %fusion.8) | copy-start | bytes 5505028
  398.2 31.4 %copy-start.1 = (bf16[1,2048,448]{1,2,0:T(8,128)(2,1)S(1)}, bf16[1,2048,448]{1,2,0:T(8,128)(2,1)}, u32[]{:S(2)}) copy-start(bf16[1,2048,448]{1,2,0:T(8,128)(2,1)} %param.22) | copy-start | bytes 5505028
Sparse Core Ops, SparseCore 0:
  54.9 33.4 all-gather.7
  98.7 33.4 all-gather.9
  266.4 20.6 all-gather.13
  289.1 49.0 all-gather.11
  342.3 87.2 reduce-scatter.1
